TPU v7x, 256 devices: a whole 4x4x8 slice. The times are simulated.
256 devices in a mesh: ep: 64 (over z, y, core), tp: 4 (over x).
Axes of the slice: x: 4, y: 4, z: 8, core: 2. Of those that a mesh axis runs over, the one named last changes fastest.
Arguments:
- first_input: bfloat16 [32768, 2048], P('ep'), may hold values from -120 to 120
- first_gain: bfloat16 [2048], replicated, may hold values from 0.099609375 to 1.8984375
- pool_inward: bfloat16 [2048, 1024], P(None, 'tp'), may hold values from -0.125 to 0.125
- pool_mixing: bfloat16 [4, 256, 256], P('tp'), may hold values from -0.375 to 0.375
- pool_scale: bfloat16 [1024], P('tp'), may hold values from 0.099609375 to 1.8984375
- pool_outward: bfloat16 [1024, 2048], P('tp'), may hold values from -0.1875 to 0.1875
- second_input: bfloat16 [16384, 2048], P('ep'), may hold values from -120 to 120
- second_gain: bfloat16 [2048], replicated, may hold values from 0.099609375 to 1.8984375
- route_ids: int32 [16384, 2], P('ep'), may hold values from 0 to 31, all different within a row; in each aligned block of 256 rows (0 to 255, 256 to 511, ...) at most 18 rows name the same one
- route_logits: float32 [16384, 2], P('ep'), may hold values from -6 to 6
- expert_gate: bfloat16 [64, 2048, 2048], P('ep', None, 'tp'), may hold values from -0.125 to 0.125
- expert_up: bfloat16 [64, 2048, 2048], P('ep', None, 'tp'), may hold values from -0.125 to 0.125
- expert_down: bfloat16 [64, 2048, 2048], P('ep', 'tp'), may hold values from -0.09375 to 0.09375
Outputs:
- first_out: bfloat16 [32768, 2048], P('ep', 'tp')
- second_out: bfloat16 [16384, 2048], P('ep', 'tp')
Inputs may be any that keep to these rules, and one draw needn't show every extreme that they name: `route_ids`: each row names two different experts. In each aligned block of 256 rows (the rows of one index of ep) no expert is named by more than 18 rows, and in some blocks one expert is named by exactly 18 rows.
All inputs are finite; a program needn't handle non-finite values.
Results may differ from a plain program's by a relative error of at most 0.012.
Values may be sent and summed in bfloat16 or wider, within the bound.
No kernel may reach another device: no remote copies, remote signals or barrier semaphores. Data moves between devices by JAX's collectives and lax.ppermute only.
A program may use at most 64 MiB of HBM per device.

v0:
```python
import jax
import jax.numpy as jnp
from jax import lax
from jax.sharding import Mesh, PartitionSpec as P

epsilon = 1e-06


def from_behind(value, axis, steps):
    count = lax.axis_size(axis)
    leading, last = (max(0, -steps), min(count, count - steps))
    return lax.ppermute(value, axis, [(source, source + steps) for source in range(leading, last)])


def rms_scaled(values, weights):
    widened = values.astype(jnp.float32)
    inverse = lax.rsqrt(jnp.mean(widened * widened, axis=-1, keepdims=True) + epsilon)
    return (widened * inverse * weights.astype(jnp.float32)).astype(jnp.bfloat16)


def window_means(channels, length, offset):
    row_count = channels.shape[0] - 15
    summed = jnp.zeros((row_count, channels.shape[1]), jnp.float32)
    for lookback in range(16):
        summed = summed + jnp.where(
            lookback < length, channels[15 - lookback : 15 - lookback + row_count], 0.0
        )
    positions = offset + jnp.arange(row_count, dtype=jnp.int32)
    counts = jnp.minimum(positions + 1, length).astype(jnp.float32)
    return summed / counts[:, None]


def slot_positions(block_ids, expert_count, capacity):
    flattened = block_ids.reshape(-1)
    onehot = (flattened[:, None] == jnp.arange(expert_count, dtype=jnp.int32)[None, :]).astype(
        jnp.int32
    )
    running = jnp.cumsum(onehot, axis=0, dtype=jnp.int32) - 1
    slot_numbers = jnp.sum(onehot * running, axis=1)
    return flattened * capacity + slot_numbers


def expert_output(gate_sum, up_sum, down_rows):
    hidden = (jax.nn.silu(gate_sum) * up_sum).astype(jnp.bfloat16)
    return jnp.dot(hidden, down_rows, preferred_element_type=jnp.float32)


def local(
    first_input,
    first_gain,
    pool_inward,
    pool_mixing,
    pool_scale,
    pool_outward,
    second_input,
    second_gain,
    route_ids,
    route_logits,
    expert_gate,
    expert_up,
    expert_down,
):
    tensor_parts = lax.axis_size("tp")
    expert_count = lax.axis_size("z") * lax.axis_size("y")
    model_width = first_input.shape[1]
    quarter_width = model_width // tensor_parts
    swap = [(0, 1), (1, 0)]
    gate_other = lax.ppermute(expert_gate[0], "core", swap)
    up_other = lax.ppermute(expert_up[0], "core", swap)
    down_other = lax.ppermute(expert_down[0], "core", swap)
    normed_first = rms_scaled(first_input, first_gain)
    pooled_in = jnp.dot(normed_first, pool_inward, preferred_element_type=jnp.float32).astype(
        jnp.bfloat16
    )
    halo_rows = from_behind(pooled_in[-15:], ("z", "y", "core"), 1)
    extended = jnp.concatenate([halo_rows, pooled_in], axis=0).astype(jnp.float32)
    window = jnp.left_shift(jnp.int32(2), lax.axis_index("tp"))
    sequence_start = lax.axis_index(("z", "y", "core")) * first_input.shape[0]
    means = window_means(extended, window, sequence_start)
    mixed = (means - pooled_in.astype(jnp.float32)).astype(jnp.bfloat16)
    pooled = (
        jnp.dot(mixed, pool_mixing[0], preferred_element_type=jnp.float32)
        * pool_scale.astype(jnp.float32)
    ).astype(jnp.bfloat16)
    mixer_term = jnp.dot(pooled, pool_outward, preferred_element_type=jnp.float32)
    normed_second = rms_scaled(second_input, second_gain)
    row_count = second_input.shape[0]
    capacity = 2 * row_count * 9 // (8 * expert_count)
    positions = slot_positions(route_ids, expert_count, capacity)
    quarter = lax.dynamic_slice_in_dim(
        normed_second, lax.axis_index("tp") * quarter_width, quarter_width, 1
    )
    repeated = jnp.repeat(quarter, 2, axis=0)
    buffer = (
        jnp.zeros((expert_count * capacity, quarter_width), jnp.bfloat16)
        .at[positions]
        .set(repeated)
        .reshape(expert_count, capacity, quarter_width)
    )
    arrived = lax.all_to_all(buffer, ("z", "y"), split_axis=0, concat_axis=0, tiled=True)
    flattened = arrived.reshape(-1, quarter_width)
    portion = lax.all_gather(flattened, "tp", axis=1, tiled=True)
    flat_term = expert_output(
        jnp.dot(portion, expert_gate[0], preferred_element_type=jnp.float32),
        jnp.dot(portion, expert_up[0], preferred_element_type=jnp.float32),
        expert_down[0],
    ) + expert_output(
        jnp.dot(portion, gate_other, preferred_element_type=jnp.float32),
        jnp.dot(portion, up_other, preferred_element_type=jnp.float32),
        down_other,
    )
    first_out = lax.psum_scatter(
        mixer_term.astype(jnp.bfloat16), "tp", scatter_dimension=1, tiled=True
    )
    expert_summed = lax.psum_scatter(
        flat_term.astype(jnp.bfloat16), "tp", scatter_dimension=1, tiled=True
    )
    half_out = expert_summed.reshape(expert_count, capacity, quarter_width)
    returned = lax.all_to_all(half_out, ("z", "y"), split_axis=0, concat_axis=0, tiled=True)
    route_out = returned.reshape(-1, quarter_width).astype(jnp.float32)
    picked = route_out[positions].reshape(row_count, 2, quarter_width)
    shares = jax.nn.sigmoid(route_logits - route_logits[:, ::-1])
    second_out = jnp.sum(picked * shares[:, :, None], axis=1).astype(jnp.bfloat16)
    return (first_out, second_out)


def solution(mesh):
    split_mesh = Mesh(mesh.devices.reshape(8, 4, 2, 4), ("z", "y", "core", "tp"))
    ep = ("z", "y", "core")
    placed = (
        P(ep, None),
        P(),
        P(None, "tp"),
        P("tp", None, None),
        P("tp"),
        P("tp", None),
        P(ep, None),
        P(),
        P(ep, None),
        P(ep, None),
        P(ep, None, "tp"),
        P(ep, None, "tp"),
        P(ep, "tp", None),
    )
    return jax.shard_map(
        local,
        mesh=split_mesh,
        in_specs=placed,
        out_specs=(P(ep, "tp"), P(ep, "tp")),
        check_vma=False,
    )
```

profile of v0, /device:TPU:8, one launch (start us, length us, event | category | flops | bytes accessed | tf_op | source)
XLA Modules:
  0.0 189.3 jit_solution(17867324479856150440)
XLA Ops:
  7.2 0.0 all-gather.2.cloned.1.call-start
  7.3 3.0 %convert_element_type.81 = f32[256,2048]{1,0:T(8,128)} convert(bf16[256,2048]{1,0:T(8,128)(2,1)} %param.19) | non-fusion elementwise | flops 524288 | bytes 3145728 | tf_op jit(solution)/shard_map/convert_element_type | solution.py:16
  10.2 0.3 multiply_reduce_fusion
  10.5 0.1 copy.17
  10.7 0.1 eq.29
  10.8 0.1 eq.25
  11.0 0.1 dynamic-slice
  11.1 1.2 fusion.16
  12.2 0.3 broadcast_in_dim.37
  12.5 0.2 reshape.116
  12.7 1.2 reduce-window.6
  13.9 0.2 slice_reduce_fusion
  14.2 0.1 copy.16
  14.3 0.1 mul.110
  14.5 0.1 fusion.75
  14.6 2.6 %scatter_custom_fusion = bf16[576,512]{1,0:T(8,128)(2,1)S(1)} fusion(s32[512]{0:T(512)S(1)} %bitcast.40, bf16[512,512]{1,0:T(8,128)(2,1)S(1)} %reshape.116, bf16[]{:T(256)} %constant.77.clone.1), kind=kCustom, calls=%fused_computation.60 | custom fusion | bytes 589826 | tf_op jit(solution)/shard_map/scatter | solution.py:97
  17.1 0.2 reshape.99
  17.3 33.9 %all_to_all.10 = bf16[32,18,512]{2,1,0:T(8,128)(2,1)S(1)} all-to-all(bf16[32,18,512]{2,1,0:T(8,128)(2,1)S(1)} %reshape.99), channel_id=1, replica_groups=mesh['z'=8,'y'=4,'core'=2,'tp'=4] {'z','y'}, dimensions={0} | all-to-all | bytes 1179648 | tf_op jit(solution)/shard_map/all_to_all | solution.py:100
  51.3 1.0 reshape.100
  52.2 0.0 all-gather.2.cloned.1.call-update
  52.3 0.0 reduce-scatter.5.cloned.1.call-start
  52.3 0.1 collective-permute-start.1
  52.4 0.5 collective-permute-start.2
  52.9 0.1 collective-permute-start.3
  53.0 31.6 %all-gather.2.cloned.1.call-done = bf16[576,2048]{1,0:T(8,128)(2,1)} async-done(((bf16[576,512]{1,0:T(8,128)(2,1)}), bf16[576,2048]{1,0:T(8,128)(2,1)}) %all-gather.2.cloned.1.call-update) | async-done | bytes 2359312 | tf_op jit(solution)/shard_map/all_gather | solution.py:102
  84.6 4.9 %fusion.80 = f32[576,512]{1,0:T(8,128)} fusion(bf16[576,2048]{1,0:T(8,128)(2,1)} %all-gather.2.cloned.1.call-done, bf16[1,2048,512]{2,1,0:T(8,128)(2,1)} %param.23), kind=kOutput, calls=%fused_computation.98 | convolution fusion | flops 1207959552 | bytes 5636096 | tf_op jit(solution)/shard_map/dot_general | solution.py:104
  89.5 4.0 %fusion.88 = f32[576,512]{1,0:T(8,128)} fusion(bf16[576,2048]{1,0:T(8,128)(2,1)S(1)} %copy-done.7, bf16[2048,512]{1,0:T(8,128)(2,1)} %collective-permute-done.1), kind=kOutput, calls=%fused_computation.104 | convolution fusion | flops 1207959552 | bytes 5636096 | tf_op jit(solution)/shard_map/dot_general | solution.py:108
  93.5 7.4 %fusion.12 = f32[576,2048]{1,0:T(8,128)} fusion(bf16[576,2048]{1,0:T(8,128)(2,1)S(1)} %copy-done.7, f32[576,512]{1,0:T(8,128)} %fusion.80, bf16[1,512,2048]{2,1,0:T(8,128)(2,1)} %param.25, bf16[1,2048,512]{2,1,0:T(8,128)(2,1)} %param.24), kind=kOutput, calls=%fused_computation.20 | convolution fusion | flops 2417688576 | bytes 12451840 | tf_op jit(solution)/shard_map/dot_general | solution.py:45
  100.9 8.1 %add_convert_fusion = bf16[576,2048]{1,0:T(8,128)(2,1)} fusion(f32[576,2048]{1,0:T(8,128)} %fusion.12, bf16[512,2048]{1,0:T(8,128)(2,1)} %collective-permute-done.3, f32[576,512]{1,0:T(8,128)} %fusion.88, bf16[576,2048]{1,0:T(8,128)(2,1)S(1)} %copy-done.7, bf16[2048,512]{1,0:T(8,128)(2,1)} %collective-permute-done.2), kind=kOutput, calls=%fused_computation.4 | convolution fusion | flops 2420047872 | bytes 14811136 | tf_op jit(solution)/shard_map/dot_general | solution.py:45
  109.1 0.0 reduce-scatter.3.cloned.1.call-start
  109.1 0.6 copy-done.5
  109.7 0.9 copy-done.2
  110.6 0.5 fusion
  111.2 0.8 fusion.8
  112.0 1.9 %collective-permute-start = (bf16[15,256]{1,0:T(8,128)(2,1)S(1)}, bf16[15,256]{1,0:T(8,128)(2,1)S(1)}, u32[]{:S(2)}, u32[]{:S(2)}) collective-permute-start(bf16[15,256]{1,0:T(8,128)(2,1)S(1)} %slice.78), channel_id=1, source_target_pairs={{0,4},{4,8},{8,12},{12,16},{16,20},{20,24},{24,28},{28,32},{32,36}... | collective-permute-start | bytes 23048 | tf_op jit(solution)/shard_map/ppermute | solution.py:12
  114.0 3.0 %collective-permute-done = bf16[15,256]{1,0:T(8,128)(2,1)S(1)} collective-permute-done((bf16[15,256]{1,0:T(8,128)(2,1)S(1)}, bf16[15,256]{1,0:T(8,128)(2,1)S(1)}, u32[]{:S(2)}, u32[]{:S(2)}) %collective-permute-start) | collective-permute-done | bytes 7712 | tf_op jit(solution)/shard_map/ppermute | solution.py:12
  116.9 0.1 maximum_convert_fusion
  117.0 3.5 %convolution_convert_fusion = bf16[512,2048]{1,0:T(8,128)(2,1)} fusion(bf16[256,2048]{1,0:T(8,128)(2,1)S(1)} %copy-done, f32[256]{0:T(256)S(1)} %convert_element_type.77, bf16[512,256]{1,0:T(8,128)(2,1)S(1)} %fusion.8, f32[527,256]{1,0:T(8,128)S(1)} %maximum_convert_fusion, f32[512]{0:T(512)S(1)} %minimum_convert_fusion, pred[]{:T(512)S(6)} %gt.63, ...), kind=kOutput, calls=%fused_computation.8 | convolution fusion | flops 609878016 | bytes 11930640 | tf_op jit(solution)/shard_map/dot_general | solution.py:85
  120.5 23.2 %reduce-scatter.5.cloned.1.call-done = bf16[576,512]{1,0:T(8,128)(2,1)} async-done(((bf16[576,2048]{1,0:T(8,128)(2,1)}), bf16[576,512]{1,0:T(8,128)(2,1)}) %reduce-scatter.5.cloned.1.call-update) | async-done | bytes 589840 | tf_op jit(solution)/shard_map/reduce_scatter | solution.py:115
  143.7 2.1 %reshape.101 = bf16[32,18,512]{2,1,0:T(8,128)(2,1)} reshape(bf16[576,512]{1,0:T(8,128)(2,1)} %reduce-scatter.5.cloned.1.call-done) | data formatting | bytes 1179648 | tf_op jit(solution)/shard_map/reshape | solution.py:118
  145.8 10.2 %all-to-all-start.1 = ((bf16[32,18,512]{2,1,0:T(8,128)(2,1)}), bf16[32,18,512]{2,1,0:T(8,128)(2,1)S(1)}, u32[]{:S(2)}, u32[]{:S(2)}) async-start(bf16[32,18,512]{2,1,0:T(8,128)(2,1)} %reshape.101), calls=%async_computation.3 | async-start | bytes 1572864 | tf_op jit(solution)/shard_map/all_to_all | solution.py:119
  156.0 0.1 rev.3
  156.1 0.1 copy.20
  156.3 22.1 %all-to-all-done.1 = bf16[32,18,512]{2,1,0:T(8,128)(2,1)S(1)} async-done(((bf16[32,18,512]{2,1,0:T(8,128)(2,1)}), bf16[32,18,512]{2,1,0:T(8,128)(2,1)S(1)}, u32[]{:S(2)}, u32[]{:S(2)}) %all-to-all-start.1) | async-done | bytes 589856 | tf_op jit(solution)/shard_map/all_to_all | solution.py:119
  178.3 0.2 reshape.103
  178.5 1.6 gather_fusion
  180.1 0.6 reshape.102
  180.8 2.1 %multiply_reduce_fusion.1 = bf16[256,512]{1,0:T(8,128)(2,1)} fusion(f32[256,2,512]{2,1,0:T(2,128)S(1)} %reshape.102, f32[256,2]{1,0:T(8,128)S(1)} %copy.20), kind=kLoop, calls=%fused_computation.19 | loop fusion | flops 393216 | bytes 1312768 | tf_op jit(solution)/shard_map/reduce_sum | solution.py:123
  (39 shorter events, 0.2 us)
Async XLA Ops:
  7.2 109.8 %copy-start = (bf16[256,2048]{1,0:T(8,128)(2,1)S(1)}, bf16[256,2048]{1,0:T(8,128)(2,1)}, u32[]{:S(2)}) copy-start(bf16[256,2048]{1,0:T(8,128)(2,1)} %param.18) | copy-start | bytes 3145732
  7.2 3.0 %copy-start.1 = (bf16[256,2048]{1,0:T(8,128)(2,1)S(1)}, bf16[256,2048]{1,0:T(8,128)(2,1)}, u32[]{:S(2)}) copy-start(bf16[256,2048]{1,0:T(8,128)(2,1)} %param.19) | copy-start | bytes 3145732
  7.2 77.5 %all-gather.2.cloned.1.call-start = ((), (), s32[]{:S(2)}) async-start(), calls=%async_computation.5 | async-start | bytes 2949120 | tf_op jit(solution)/shard_map/all_gather | solution.py:102
  7.2 3.3 %copy-start.3 = (s32[256,2]{0,1:T(2,128)S(1)}, s32[256,2]{0,1:T(2,128)}, u32[]{:S(2)}) copy-start(s32[256,2]{0,1:T(2,128)} %param.21) | copy-start | bytes 6148
  7.2 3.7 %copy-start.6 = (bf16[2048]{0:T(1024)(128)(2,1)S(1)}, bf16[2048]{0:T(1024)(128)(2,1)}, u32[]{:S(2)}) copy-start(bf16[2048]{0:T(1024)(128)(2,1)} %param.20) | copy-start | bytes 12292
  52.3 91.4 %reduce-scatter.5.cloned.1.call-start = ((), (), s32[]{:S(2)}) async-start(), calls=%async_computation.6 | async-start | bytes 2949120 | tf_op jit(solution)/shard_map/reduce_scatter | solution.py:115
  52.3 37.2 %collective-permute-start.1 = (bf16[2048,512]{1,0:T(8,128)(2,1)}, bf16[2048,512]{1,0:T(8,128)(2,1)}, u32[]{:S(2)}, u32[]{:S(2)}) collective-permute-start(bf16[2048,512]{1,0:T(8,128)(2,1)} %bitcast.43), channel_id=1, source_target_pairs={{0,4},{4,0},{1,5},{5,1},{2,6},{6,2},{3,7},{7,3},{8,12},{12,8},{9,1... | collective-permute-start | bytes 6291464 | tf_op jit(solution)/shard_map/ppermute | solution.py:68
  52.4 48.5 %collective-permute-start.2 = (bf16[2048,512]{1,0:T(8,128)(2,1)}, bf16[2048,512]{1,0:T(8,128)(2,1)}, u32[]{:S(2)}, u32[]{:S(2)}) collective-permute-start(bf16[2048,512]{1,0:T(8,128)(2,1)} %bitcast.44), channel_id=1, source_target_pairs={{0,4},{4,0},{1,5},{5,1},{2,6},{6,2},{3,7},{7,3},{8,12},{12,8},{9,1... | collective-permute-start | bytes 6291464 | tf_op jit(solution)/shard_map/ppermute | solution.py:69
  52.9 48.0 %collective-permute-start.3 = (bf16[512,2048]{1,0:T(8,128)(2,1)}, bf16[512,2048]{1,0:T(8,128)(2,1)}, u32[]{:S(2)}, u32[]{:S(2)}) collective-permute-start(bf16[512,2048]{1,0:T(8,128)(2,1)} %bitcast.45), channel_id=1, source_target_pairs={{0,4},{4,0},{1,5},{5,1},{2,6},{6,2},{3,7},{7,3},{8,12},{12,8},{9,1... | collective-permute-start | bytes 6291464 | tf_op jit(solution)/shard_map/ppermute | solution.py:70
  84.6 4.9 %copy-start.7 = (bf16[576,2048]{1,0:T(8,128)(2,1)S(1)}, bf16[576,2048]{1,0:T(8,128)(2,1)}, u32[]{:S(2)}) copy-start(bf16[576,2048]{1,0:T(8,128)(2,1)} %all-gather.2.cloned.1.call-done) | copy-start | bytes 7077892
  109.0 0.7 copy-start.5
  109.0 1.6 copy-start.2
  109.1 73.8 %reduce-scatter.3.cloned.1.call-start = ((), (), s32[]{:S(2)}) async-start(), calls=%async_computation.4 | async-start | bytes 2621440 | tf_op jit(solution)/shard_map/reduce_scatter | solution.py:112
  109.7 1.4 copy-start.8
  111.1 2.8 %copy-start.10 = (bf16[256]{0:T(256)(128)(2,1)S(1)}, bf16[256]{0:T(256)(128)(2,1)}, u32[]{:S(2)}) copy-start(bf16[256]{0:T(256)(128)(2,1)} %param.17) | copy-start | bytes 1540
  111.2 5.9 %copy-start.9 = (bf16[1,256,256]{2,1,0:T(8,128)(2,1)S(1)}, bf16[1,256,256]{2,1,0:T(8,128)(2,1)}, u32[]{:S(2)}) copy-start(bf16[1,256,256]{2,1,0:T(8,128)(2,1)} %param.16) | copy-start | bytes 393220
  112.0 5.0 %collective-permute-start = (bf16[15,256]{1,0:T(8,128)(2,1)S(1)}, bf16[15,256]{1,0:T(8,128)(2,1)S(1)}, u32[]{:S(2)}, u32[]{:S(2)}) collective-permute-start(bf16[15,256]{1,0:T(8,128)(2,1)S(1)} %slice.78), channel_id=1, source_target_pairs={{0,4},{4,8},{8,12},{12,16},{16,20},{20,24},{24,28},{28,32},{32,36}... | collective-permute-start | bytes 23048 | tf_op jit(solution)/shard_map/ppermute | solution.py:12
  120.5 35.5 %copy-start.4 = (f32[256,2]{0,1:T(2,128)S(1)}, f32[256,2]{0,1:T(2,128)}, u32[]{:S(2)}) copy-start(f32[256,2]{0,1:T(2,128)} %param.22) | copy-start | bytes 6148
  145.8 32.5 %all-to-all-start.1 = ((bf16[32,18,512]{2,1,0:T(8,128)(2,1)}), bf16[32,18,512]{2,1,0:T(8,128)(2,1)S(1)}, u32[]{:S(2)}, u32[]{:S(2)}) async-start(bf16[32,18,512]{2,1,0:T(8,128)(2,1)} %reshape.101), calls=%async_computation.3 | async-start | bytes 1572864 | tf_op jit(solution)/shard_map/all_to_all | solution.py:119
Sparse Core Ops, SparseCore 0:
  52.4 32.2 all-gather.1
  109.2 34.4 reduce-scatter.4
  146.8 31.9 reduce-scatter.2
where the time goes:
time: 190 us; the launch traced here: 189 us
  waiting for transfers between devices  79.9 us (42%)
  blocking collectives  33.9 us (18%)
  matrix products  28.7 us (15%)
  between operations  14.1 us (7%)
  starting transfers between devices  12.9 us (7%)
  local copies, waits for them, and re-layouts  11.5 us (6%)
  other arithmetic  8.35 us (4%)
    all_to_all x1, blocking collectives, local(): lax.all_to_all(buffer, ('z', 'y'), split_axis=0, concat_axis=0, tiled=True)  33.9 us
    all_gather x1, waiting for transfers between devices, local(): portion = lax.all_gather(flattened, 'tp', axis=1, tiled=True)  31.6 us
    reduce_scatter x1, waiting for transfers between devices, local(): lax.psum_scatter(flat_term.astype(jnp.bfloat16), 'tp', scatter_dimension=...  23.2 us
    all_to_all x1, waiting for transfers between devices, local(): lax.all_to_all(half_out, ('z', 'y'), split_axis=0, concat_axis=0, tiled=T...  22.1 us
    dot_general x2, matrix products, expert_output(): return jnp.dot(hidden, down_rows, preferred_element_type=jnp.float32)  15.5 us
    all_to_all x1, starting transfers between devices, local(): lax.all_to_all(half_out, ('z', 'y'), split_axis=0, concat_axis=0, tiled=T...  10.2 us
    dot_general x1, matrix products, local(): jnp.dot(portion, expert_gate[0], preferred_element_type=jnp.float32)  4.89 us
    dot_general x1, matrix products, local(): jnp.dot(portion, gate_other, preferred_element_type=jnp.float32)  3.97 us
  transfers between devices with their start and end apart: 8, of which 4 were waited for; matrix products, arithmetic and copies ran while one was open for 15% of the time, Pallas kernels for 0%

commit v1 on v0

--- a/solution.py
+++ b/solution.py
@@ -99,7 +99,8 @@
     )
     arrived = lax.all_to_all(buffer, ("z", "y"), split_axis=0, concat_axis=0, tiled=True)
     flattened = arrived.reshape(-1, quarter_width)
-    portion = lax.all_gather(flattened, "tp", axis=1, tiled=True)
+    copies = jnp.concatenate([flattened] * lax.axis_size("tp"), axis=1)
+    portion = lax.all_to_all(copies, "tp", 1, 1, tiled=True)
     flat_term = expert_output(
         jnp.dot(portion, expert_gate[0], preferred_element_type=jnp.float32),
         jnp.dot(portion, expert_up[0], preferred_element_type=jnp.float32),

time: 190 us -> 184 us (0.968)
  waiting for transfers between devices: 79.9 us -> 70.4 us
  starting transfers between devices: 12.9 us -> 17 us
  local copies, waits for them, and re-layouts: 11.5 us -> 14.7 us
  other arithmetic: 8.35 us -> 5.95 us
    all_gather x1 -> x0, waiting for transfers between devices: 31.6 us -> none  [local(): portion = lax.all_gather(flattened, 'tp', axis=1, tiled=True)]
    all_to_all x0 -> x1, waiting for transfers between devices: none -> 26.9 us  [local(): portion = lax.all_to_all(copies, 'tp', 1, 1, tiled=True)]
    reduce_scatter x1, waiting for transfers between devices: 23.2 us -> 18.4 us  [local(): lax.psum_scatter(flat_term.astype(jnp.bfloat16), 'tp', scatter_dimension=...]
    all_to_all x0 -> x1, starting transfers between devices: none -> 4.29 us  [local(): portion = lax.all_to_all(copies, 'tp', 1, 1, tiled=True)]
    dot_general x1, matrix products: 4.89 us -> 2.47 us  [local(): jnp.dot(portion, expert_gate[0], preferred_element_type=jnp.float32)]
    unnamed x23 -> x27, local copies, waits for them, and re-layouts: 1.71 us -> 3.81 us
where the time goes in v1:
time: 184 us
  waiting for transfers between devices  70.4 us (38%)
  blocking collectives  33.9 us (18%)
  matrix products  27.1 us (15%)
  starting transfers between devices  17 us (9%)
  local copies, waits for them, and re-layouts  14.7 us (8%)
  between operations  14.4 us (8%)
  other arithmetic  5.95 us (3%)
    all_to_all x1, blocking collectives, local(): lax.all_to_all(buffer, ('z', 'y'), split_axis=0, concat_axis=0, tiled=True)  33.9 us
    all_to_all x1, waiting for transfers between devices, local(): portion = lax.all_to_all(copies, 'tp', 1, 1, tiled=True)  26.9 us
    all_to_all x1, waiting for transfers between devices, local(): lax.all_to_all(half_out, ('z', 'y'), split_axis=0, concat_axis=0, tiled=T...  22.1 us
    reduce_scatter x1, waiting for transfers between devices, local(): lax.psum_scatter(flat_term.astype(jnp.bfloat16), 'tp', scatter_dimension=...  18.4 us
    dot_general x2, matrix products, expert_output(): return jnp.dot(hidden, down_rows, preferred_element_type=jnp.float32)  16.4 us
    all_to_all x1, starting transfers between devices, local(): lax.all_to_all(half_out, ('z', 'y'), split_axis=0, concat_axis=0, tiled=T...  10.2 us
    all_to_all x1, starting transfers between devices, local(): portion = lax.all_to_all(copies, 'tp', 1, 1, tiled=True)  4.29 us
    dot_general x1, matrix products, local(): jnp.dot(portion, gate_other, preferred_element_type=jnp.float32)  3.99 us
  transfers between devices with their start and end apart: 8, of which 4 were waited for; matrix products, arithmetic and copies ran while one was open for 15% of the time, Pallas kernels for 0%

profile of v1, /device:TPU:8, one launch (start us, length us, event | category | flops | bytes accessed | tf_op | source)
XLA Modules:
  0.0 183.6 jit_solution(6292548652725823668)
XLA Ops:
  7.2 1.6 convert_element_type.81
  8.8 0.3 multiply_reduce_fusion
  9.1 0.1 copy.27
  9.3 0.1 eq.29
  9.4 0.1 eq.25
  9.6 0.1 dynamic-slice
  9.7 0.1 fusion.16
  9.8 0.3 broadcast_in_dim.37
  10.1 0.2 reshape.125
  10.3 1.2 reduce-window.6
  11.5 0.2 slice_reduce_fusion
  11.7 0.1 copy.26
  11.9 0.1 mul.110
  12.0 0.1 fusion.75
  12.1 2.6 %scatter_custom_fusion = bf16[576,512]{1,0:T(8,128)(2,1)S(1)} fusion(s32[512]{0:T(512)S(1)} %bitcast.47, bf16[512,512]{1,0:T(8,128)(2,1)S(1)} %reshape.125, bf16[]{:T(256)} %constant.77.clone.1), kind=kCustom, calls=%fused_computation.60 | custom fusion | bytes 589826 | tf_op jit(solution)/shard_map/scatter | solution.py:97
  14.7 0.2 reshape.109
  14.9 33.9 %all_to_all.19 = bf16[32,18,512]{2,1,0:T(8,128)(2,1)S(1)} all-to-all(bf16[32,18,512]{2,1,0:T(8,128)(2,1)S(1)} %reshape.109), channel_id=1, replica_groups=mesh['z'=8,'y'=4,'core'=2,'tp'=4] {'z','y'}, dimensions={0} | all-to-all | bytes 1179648 | tf_op jit(solution)/shard_map/all_to_all | solution.py:100
  48.8 0.2 concatenate.10
  49.0 1.6 concatenate.11
  50.6 4.3 %all-to-all-start.1 = ((bf16[576,4,512]{2,0,1:T(8,128)(2,1)}), bf16[576,4,512]{2,0,1:T(8,128)(2,1)S(1)}, u32[]{:S(2)}, u32[]{:S(2)}) async-start(bf16[576,4,512]{2,0,1:T(8,128)(2,1)} %concatenate.11), calls=%async_computation.2 | async-start | bytes 4718592 | tf_op jit(solution)/shard_map/all_to_all | solution.py:103
  54.9 0.5 collective-permute-start.2
  55.4 0.1 collective-permute-start.3
  55.5 26.9 %all-to-all-done.1 = bf16[576,4,512]{2,0,1:T(8,128)(2,1)S(1)} async-done(((bf16[576,4,512]{2,0,1:T(8,128)(2,1)}), bf16[576,4,512]{2,0,1:T(8,128)(2,1)S(1)}, u32[]{:S(2)}, u32[]{:S(2)}) %all-to-all-start.1) | async-done | bytes 2359328 | tf_op jit(solution)/shard_map/all_to_all | solution.py:103
  82.4 0.3 copy.33
  82.7 2.1 %copy-done.9 = bf16[1,2048,512]{2,1,0:T(8,128)(2,1)S(1)} copy-done((bf16[1,2048,512]{2,1,0:T(8,128)(2,1)S(1)}, bf16[1,2048,512]{2,1,0:T(8,128)(2,1)}, u32[]{:S(2)}) %copy-start.9) | copy-done | bytes 2097176
  84.8 2.5 %fusion.80 = f32[576,512]{1,0:T(8,128)} fusion(bf16[576,2048]{1,0:T(8,128)(2,1)S(1)} %bitcast.43, bf16[1,2048,512]{2,1,0:T(8,128)(2,1)S(1)} %copy-done.9), kind=kOutput, calls=%fused_computation.98 | convolution fusion | flops 1207959552 | bytes 5636096 | tf_op jit(solution)/shard_map/dot_general | solution.py:105
  87.3 4.0 %fusion.88 = f32[576,512]{1,0:T(8,128)} fusion(bf16[576,2048]{1,0:T(8,128)(2,1)S(1)} %bitcast.44, bf16[2048,512]{1,0:T(8,128)(2,1)} %collective-permute-done.1), kind=kOutput, calls=%fused_computation.104 | convolution fusion | flops 1207959552 | bytes 5636096 | tf_op jit(solution)/shard_map/dot_general | solution.py:109
  91.3 8.3 %fusion.12 = f32[576,2048]{1,0:T(8,128)} fusion(bf16[576,2048]{1,0:T(8,128)(2,1)} %bitcast.45, f32[576,512]{1,0:T(8,128)} %fusion.80, bf16[1,512,2048]{2,1,0:T(8,128)(2,1)} %param.25, bf16[1,2048,512]{2,1,0:T(8,128)(2,1)} %param.24), kind=kOutput, calls=%fused_computation.20 | convolution fusion | flops 2417688576 | bytes 12451840 | tf_op jit(solution)/shard_map/dot_general | solution.py:45
  99.6 8.1 %add_convert_fusion = bf16[576,2048]{1,0:T(8,128)(2,1)} fusion(f32[576,2048]{1,0:T(8,128)} %fusion.12, bf16[512,2048]{1,0:T(8,128)(2,1)} %collective-permute-done.3, f32[576,512]{1,0:T(8,128)} %fusion.88, bf16[576,2048]{1,0:T(8,128)(2,1)S(1)} %bitcast.46, bf16[2048,512]{1,0:T(8,128)(2,1)} %collective-permute-done.2), kind=kOutput, calls=%fused_computation.4 | convolution fusion | flops 2420047872 | bytes 14811136 | tf_op jit(solution)/shard_map/dot_general | solution.py:45
  107.7 0.0 reduce-scatter.3.cloned.1.call-start
  107.7 0.6 copy-done.7
  108.4 0.9 copy-done.4
  109.3 0.5 fusion
  109.8 0.8 fusion.8
  110.6 1.9 %collective-permute-start = (bf16[15,256]{1,0:T(8,128)(2,1)S(1)}, bf16[15,256]{1,0:T(8,128)(2,1)S(1)}, u32[]{:S(2)}, u32[]{:S(2)}) collective-permute-start(bf16[15,256]{1,0:T(8,128)(2,1)S(1)} %slice.78), channel_id=1, source_target_pairs={{0,4},{4,8},{8,12},{12,16},{16,20},{20,24},{24,28},{28,32},{32,36}... | collective-permute-start | bytes 23048 | tf_op jit(solution)/shard_map/ppermute | solution.py:12
  112.6 3.0 %collective-permute-done = bf16[15,256]{1,0:T(8,128)(2,1)S(1)} collective-permute-done((bf16[15,256]{1,0:T(8,128)(2,1)S(1)}, bf16[15,256]{1,0:T(8,128)(2,1)S(1)}, u32[]{:S(2)}, u32[]{:S(2)}) %collective-permute-start) | collective-permute-done | bytes 7712 | tf_op jit(solution)/shard_map/ppermute | solution.py:12
  115.6 0.1 maximum_convert_fusion
  115.7 3.5 %convolution_convert_fusion = bf16[512,2048]{1,0:T(8,128)(2,1)} fusion(bf16[256,2048]{1,0:T(8,128)(2,1)S(1)} %copy-done, f32[256]{0:T(256)S(1)} %convert_element_type.77, bf16[512,256]{1,0:T(8,128)(2,1)S(1)} %fusion.8, f32[527,256]{1,0:T(8,128)S(1)} %maximum_convert_fusion, f32[512]{0:T(512)S(1)} %minimum_convert_fusion, pred[]{:T(512)S(6)} %gt.63, ...), kind=kOutput, calls=%fused_computation.8 | convolution fusion | flops 609878016 | bytes 11930640 | tf_op jit(solution)/shard_map/dot_general | solution.py:85
  119.2 18.4 %reduce-scatter.5.cloned.1.call-done = bf16[576,512]{1,0:T(8,128)(2,1)} async-done(((bf16[576,2048]{1,0:T(8,128)(2,1)}), bf16[576,512]{1,0:T(8,128)(2,1)}) %reduce-scatter.5.cloned.1.call-update) | async-done | bytes 589840 | tf_op jit(solution)/shard_map/reduce_scatter | solution.py:116
  137.6 2.1 %reshape.110 = bf16[32,18,512]{2,1,0:T(8,128)(2,1)} reshape(bf16[576,512]{1,0:T(8,128)(2,1)} %reduce-scatter.5.cloned.1.call-done) | data formatting | bytes 1179648 | tf_op jit(solution)/shard_map/reshape | solution.py:119
  139.7 10.2 %all-to-all-start.2 = ((bf16[32,18,512]{2,1,0:T(8,128)(2,1)}), bf16[32,18,512]{2,1,0:T(8,128)(2,1)S(1)}, u32[]{:S(2)}, u32[]{:S(2)}) async-start(bf16[32,18,512]{2,1,0:T(8,128)(2,1)} %reshape.110), calls=%async_computation.4 | async-start | bytes 1572864 | tf_op jit(solution)/shard_map/all_to_all | solution.py:120
  149.9 0.1 rev.3
  150.0 0.1 copy.31
  150.1 22.1 %all-to-all-done.2 = bf16[32,18,512]{2,1,0:T(8,128)(2,1)S(1)} async-done(((bf16[32,18,512]{2,1,0:T(8,128)(2,1)}), bf16[32,18,512]{2,1,0:T(8,128)(2,1)S(1)}, u32[]{:S(2)}, u32[]{:S(2)}) %all-to-all-start.2) | async-done | bytes 589856 | tf_op jit(solution)/shard_map/all_to_all | solution.py:120
  172.2 0.2 reshape.112
  172.4 1.6 gather_fusion
  174.0 0.6 reshape.111
  174.7 2.1 %multiply_reduce_fusion.1 = bf16[256,512]{1,0:T(8,128)(2,1)} fusion(f32[256,2,512]{2,1,0:T(2,128)S(1)} %reshape.111, f32[256,2]{1,0:T(8,128)S(1)} %copy.31), kind=kLoop, calls=%fused_computation.19 | loop fusion | flops 393216 | bytes 1312768 | tf_op jit(solution)/shard_map/reduce_sum | solution.py:124
  (44 shorter events, 0.2 us)
Async XLA Ops:
  7.2 108.5 %copy-start = (bf16[256,2048]{1,0:T(8,128)(2,1)S(1)}, bf16[256,2048]{1,0:T(8,128)(2,1)}, u32[]{:S(2)}) copy-start(bf16[256,2048]{1,0:T(8,128)(2,1)} %param.18) | copy-start | bytes 3145732
  7.2 1.6 copy-start.1
  7.2 1.9 %copy-start.5 = (s32[256,2]{0,1:T(2,128)S(1)}, s32[256,2]{0,1:T(2,128)}, u32[]{:S(2)}) copy-start(s32[256,2]{0,1:T(2,128)} %param.21) | copy-start | bytes 6148
  7.2 2.4 %copy-start.8 = (bf16[2048]{0:T(1024)(128)(2,1)S(1)}, bf16[2048]{0:T(1024)(128)(2,1)}, u32[]{:S(2)}) copy-start(bf16[2048]{0:T(1024)(128)(2,1)} %param.20) | copy-start | bytes 12292
  50.6 31.8 %all-to-all-start.1 = ((bf16[576,4,512]{2,0,1:T(8,128)(2,1)}), bf16[576,4,512]{2,0,1:T(8,128)(2,1)S(1)}, u32[]{:S(2)}, u32[]{:S(2)}) async-start(bf16[576,4,512]{2,0,1:T(8,128)(2,1)} %concatenate.11), calls=%async_computation.2 | async-start | bytes 4718592 | tf_op jit(solution)/shard_map/all_to_all | solution.py:103
  54.9 82.7 %reduce-scatter.5.cloned.1.call-start = ((), (), s32[]{:S(2)}) async-start(), calls=%async_computation.6 | async-start | bytes 2949120 | tf_op jit(solution)/shard_map/reduce_scatter | solution.py:116
  54.9 32.4 %collective-permute-start.1 = (bf16[2048,512]{1,0:T(8,128)(2,1)}, bf16[2048,512]{1,0:T(8,128)(2,1)}, u32[]{:S(2)}, u32[]{:S(2)}) collective-permute-start(bf16[2048,512]{1,0:T(8,128)(2,1)} %bitcast.50), channel_id=1, source_target_pairs={{0,4},{4,0},{1,5},{5,1},{2,6},{6,2},{3,7},{7,3},{8,12},{12,8},{9,1... | collective-permute-start | bytes 6291464 | tf_op jit(solution)/shard_map/ppermute | solution.py:68
  54.9 44.6 %collective-permute-start.2 = (bf16[2048,512]{1,0:T(8,128)(2,1)}, bf16[2048,512]{1,0:T(8,128)(2,1)}, u32[]{:S(2)}, u32[]{:S(2)}) collective-permute-start(bf16[2048,512]{1,0:T(8,128)(2,1)} %bitcast.51), channel_id=1, source_target_pairs={{0,4},{4,0},{1,5},{5,1},{2,6},{6,2},{3,7},{7,3},{8,12},{12,8},{9,1... | collective-permute-start | bytes 6291464 | tf_op jit(solution)/shard_map/ppermute | solution.py:69
  55.4 44.1 %collective-permute-start.3 = (bf16[512,2048]{1,0:T(8,128)(2,1)}, bf16[512,2048]{1,0:T(8,128)(2,1)}, u32[]{:S(2)}, u32[]{:S(2)}) collective-permute-start(bf16[512,2048]{1,0:T(8,128)(2,1)} %bitcast.52), channel_id=1, source_target_pairs={{0,4},{4,0},{1,5},{5,1},{2,6},{6,2},{3,7},{7,3},{8,12},{12,8},{9,1... | collective-permute-start | bytes 6291464 | tf_op jit(solution)/shard_map/ppermute | solution.py:70
  82.4 2.4 %copy-start.9 = (bf16[1,2048,512]{2,1,0:T(8,128)(2,1)S(1)}, bf16[1,2048,512]{2,1,0:T(8,128)(2,1)}, u32[]{:S(2)}) copy-start(bf16[1,2048,512]{2,1,0:T(8,128)(2,1)} %param.23) | copy-start | bytes 6291460
  82.7 4.6 %copy-start.2 = (bf16[4,72,8,512]{3,2,0,1:T(8,128)(2,1)}, bf16[4,72,8,512]{3,2,0,1:T(8,128)(2,1)S(1)}, u32[]{:S(2)}) copy-start(bf16[4,72,8,512]{3,2,0,1:T(8,128)(2,1)S(1)} %copy.33) | copy-start | bytes 7077892
  91.3 8.3 %copy-start.3 = (bf16[4,72,8,512]{3,2,0,1:T(8,128)(2,1)S(1)}, bf16[4,72,8,512]{3,2,0,1:T(8,128)(2,1)}, u32[]{:S(2)}) copy-start(bf16[4,72,8,512]{3,2,0,1:T(8,128)(2,1)} %copy-done.2) | copy-start | bytes 7077892
  107.7 0.7 copy-start.7
  107.7 1.6 copy-start.4
  107.7 69.0 %reduce-scatter.3.cloned.1.call-start = ((), (), s32[]{:S(2)}) async-start(), calls=%async_computation.5 | async-start | bytes 2621440 | tf_op jit(solution)/shard_map/reduce_scatter | solution.py:113
  108.4 1.4 copy-start.10
  109.8 2.8 %copy-start.12 = (bf16[256]{0:T(256)(128)(2,1)S(1)}, bf16[256]{0:T(256)(128)(2,1)}, u32[]{:S(2)}) copy-start(bf16[256]{0:T(256)(128)(2,1)} %param.17) | copy-start | bytes 1540
  109.8 5.9 %copy-start.11 = (bf16[1,256,256]{2,1,0:T(8,128)(2,1)S(1)}, bf16[1,256,256]{2,1,0:T(8,128)(2,1)}, u32[]{:S(2)}) copy-start(bf16[1,256,256]{2,1,0:T(8,128)(2,1)} %param.16) | copy-start | bytes 393220
  110.6 5.0 %collective-permute-start = (bf16[15,256]{1,0:T(8,128)(2,1)S(1)}, bf16[15,256]{1,0:T(8,128)(2,1)S(1)}, u32[]{:S(2)}, u32[]{:S(2)}) collective-permute-start(bf16[15,256]{1,0:T(8,128)(2,1)S(1)} %slice.78), channel_id=1, source_target_pairs={{0,4},{4,8},{8,12},{12,16},{16,20},{20,24},{24,28},{28,32},{32,36}... | collective-permute-start | bytes 23048 | tf_op jit(solution)/shard_map/ppermute | solution.py:12
  119.2 30.7 %copy-start.6 = (f32[256,2]{0,1:T(2,128)S(1)}, f32[256,2]{0,1:T(2,128)}, u32[]{:S(2)}) copy-start(f32[256,2]{0,1:T(2,128)} %param.22) | copy-start | bytes 6148
  139.7 32.5 %all-to-all-start.2 = ((bf16[32,18,512]{2,1,0:T(8,128)(2,1)}), bf16[32,18,512]{2,1,0:T(8,128)(2,1)S(1)}, u32[]{:S(2)}, u32[]{:S(2)}) async-start(bf16[32,18,512]{2,1,0:T(8,128)(2,1)} %reshape.110), calls=%async_computation.4 | async-start | bytes 1572864 | tf_op jit(solution)/shard_map/all_to_all | solution.py:120
Sparse Core Ops, SparseCore 0:
  107.8 29.7 reduce-scatter.4
  140.7 32.0 reduce-scatter.2
